TPU v7x, 512 devices: a whole 4x8x8 slice. The times are simulated.
512 devices in a mesh: sp: 128 (over z, y, core), tp: 4 (over x).
Axes of the slice: x: 4, y: 8, z: 8, core: 2. Of those that a mesh axis runs over, the one named last changes fastest.
Arguments:
- tokens: bfloat16 [16384, 2048], P(('sp', 'tp')), may hold values from -8.5 to 8.5
- norm_gain: bfloat16 [2048], replicated, may hold values from 0.099609375 to 1.8984375
- w_query: bfloat16 [2048, 1024], P(None, 'tp'), may hold values from -0.088388348 to 0.088388348
- w_key: bfloat16 [2048, 512], P(None, 'tp'), may hold values from -5.3298174 to 5.3298174
- w_value: bfloat16 [2048, 512], P(None, 'tp'), may hold values from -0.125 to 0.125
- w_conv_value: bfloat16 [2048, 1024], P(None, 'tp'), may hold values from -0.125 to 0.125
- w_conv_gate: bfloat16 [2048, 1024], P(None, 'tp'), may hold values from -0.125 to 0.125
- conv_taps: bfloat16 [31, 1024], P(None, 'tp'), may hold values from -1 to 1
- conv_gain: bfloat16 [1024], P('tp'), may hold values from 0.099609375 to 1.8984375
- conv_bias: bfloat16 [1024], P('tp'), may hold values from -3 to 3
- cum_gate: float32 [16384, 8], P(None, 'tp'), may hold values from -1969 to 0, as said below
- w_out_att: bfloat16 [1024, 2048], P('tp', 'sp'), may hold values from -0.28125 to 0.28125
- w_out_conv: bfloat16 [1024, 2048], P('tp', 'sp'), may hold values from -0.1875 to 0.1875
Outputs:
- mixed_out: bfloat16 [16384, 2048], P('sp', 'tp')
Inputs may be any that keep to these rules, and one draw needn't show every extreme that they name: `cum_gate`: in each head, non-increasing along positions, and at most 0.
All inputs are finite; a program needn't handle non-finite values.
Results may differ from a plain program's by a relative error of at most 0.012.
Values may be sent and summed in bfloat16 or wider, within the bound.
A program may use at most 64 MiB of HBM per device.

v0:
```python
import math

import jax
import jax.numpy as jnp
from jax import lax
from jax.sharding import PartitionSpec as P

HEAD = 128
CONV = 1024
KW = 31


def joined_along(blocks, dim):
    blocks = jnp.moveaxis(blocks, 0, dim)
    shape = blocks.shape
    return blocks.reshape(*shape[:dim], shape[dim] * shape[dim + 1], *shape[dim + 2 :])


def sent_to_all(array, axis):
    copies = jnp.broadcast_to(array, (lax.axis_size(axis), *array.shape))
    return lax.all_to_all(copies, axis, split_axis=0, concat_axis=0, tiled=True)


def gathered_copies(array, axis, dim):
    return joined_along(sent_to_all(array, axis), dim)


def sent_together(arrays, axis, dim, along):
    widths = [a.shape[along] for a in arrays]
    both = jnp.concatenate(arrays, axis=along)
    out = lax.all_gather(both, axis, axis=dim, tiled=True)
    return tuple(jnp.split(out, [sum(widths[:k]) for k in range(1, len(widths))], axis=along))


def shifted(array, axis, by):
    peers = lax.axis_size(axis)
    pairs = [(i, i + by) for i in range(peers) if 0 <= i + by < peers]
    return lax.ppermute(array, axis, pairs)


def taken_together(array, axis):
    everything = sent_to_all(array, axis)
    return jnp.sum(everything, axis=0)


def in_one(arrays, axis):
    ends = [0]
    for a in arrays:
        ends.append(ends[-1] + a.size)
    total = taken_together(jnp.concatenate([a.ravel() for a in arrays]), axis)
    return tuple((total[b:e].reshape(a.shape) for a, b, e in zip(arrays, ends, ends[1:])))


def gather_turned(arrays, axis, dims):
    turned = [jnp.moveaxis(a, dim, 0) for a, dim in zip(arrays, dims)]
    both = jnp.concatenate([t.reshape(len(t), -1) for t in turned], axis=1)
    out, at, finished = (lax.all_gather(both, axis, axis=0, tiled=True), 0, [])
    for t, dim in zip(turned, dims):
        share = out[:, at : at + t[0].size].reshape(-1, *t.shape[1:])
        finished.append(jnp.moveaxis(share, 0, dim))
        at += t[0].size
    return tuple(finished)


def cut_along(array, dim, peers):
    before, after = (array.shape[:dim], array.shape[dim + 1 :])
    return jnp.moveaxis(array.reshape(*before, peers, -1, *after), dim, 0)


def sum_at_owner(array, axis, dim):
    blocks = cut_along(array, dim, lax.axis_size(axis))
    arrived = lax.all_to_all(blocks, axis, split_axis=0, concat_axis=0, tiled=True)
    return arrived.astype(jnp.float32).sum(axis=0)


def shards(
    tokens,
    norm_gain,
    w_query,
    w_key,
    w_value,
    w_conv_value,
    w_conv_gate,
    conv_taps,
    conv_gain,
    conv_bias,
    cum_gate,
    w_out_att,
    w_out_conv,
):
    query_cols = w_query.shape[1]
    kv_cols = w_key.shape[1]
    conv_cols = w_conv_value.shape[1]
    head_count = query_cols // HEAD
    kv_count = kv_cols // HEAD
    group_size = head_count // kv_count
    gain_float = norm_gain.astype(jnp.float32)
    floats = gathered_copies(tokens, "tp", 0).astype(jnp.float32)
    normed = (
        floats * lax.rsqrt(jnp.mean(floats * floats, axis=-1, keepdims=True) + 1e-06) * gain_float
    ).astype(jnp.bfloat16)
    query_part = jnp.dot(normed, w_query, preferred_element_type=jnp.float32).astype(jnp.bfloat16)
    key_part = jnp.dot(normed, w_key, preferred_element_type=jnp.float32).astype(jnp.bfloat16)
    value_part = jnp.dot(normed, w_value, preferred_element_type=jnp.float32).astype(jnp.bfloat16)
    value_glu = jnp.dot(normed, w_conv_value, preferred_element_type=jnp.float32)
    gate_glu = jnp.dot(normed, w_conv_gate, preferred_element_type=jnp.float32)
    glu_part = (value_glu * jax.nn.sigmoid(gate_glu)).astype(jnp.bfloat16)
    joined = jnp.concatenate([query_part, key_part, value_part, glu_part], axis=1)
    local_rows = joined.shape[0]
    query = joined[:, :query_cols]
    key_rows = joined[:, query_cols : query_cols + kv_cols]
    value_rows = joined[:, query_cols + kv_cols : query_cols + 2 * kv_cols]
    glu = joined[:, query_cols + 2 * kv_cols :]
    offset = lax.axis_index("sp") * local_rows
    query_places = offset + jnp.arange(local_rows, dtype=jnp.int32)
    query_gate = lax.dynamic_slice_in_dim(cum_gate, offset, local_rows, 0).T
    query_groups = query.reshape(local_rows, kv_count, group_size, HEAD)
    scale = 1.0 / math.sqrt(HEAD)

    def attend_block(state, key_block, value_block, key_start):
        run_max, run_sum, run_acc = state
        span = key_block.shape[0]
        key_heads = key_block.reshape(span, kv_count, HEAD)
        value_heads = value_block.reshape(span, kv_count, HEAD)
        scores = (
            jnp.einsum(
                "tkgd,skd->kgts", query_groups, key_heads, preferred_element_type=jnp.float32
            ).reshape(head_count, local_rows, span)
            * scale
        )
        key_gate = lax.dynamic_slice_in_dim(cum_gate, key_start, span, 0).T
        logits = scores + query_gate[:, :, None] - key_gate[:, None, :]
        key_places = key_start + jnp.arange(span, dtype=jnp.int32)
        allowed = (key_places[None, :] <= query_places[:, None])[None]
        logits = jnp.where(allowed, logits, -1e30)
        new_max = jnp.maximum(run_max, jnp.max(logits, axis=-1))
        weights = jnp.where(allowed, jnp.exp(logits - new_max[:, :, None]), 0.0)
        factor = jnp.exp(run_max - new_max)
        new_sum = run_sum * factor + jnp.sum(weights, axis=-1)
        grouped = weights.astype(jnp.bfloat16).reshape(kv_count, group_size, local_rows, span)
        product = jnp.einsum(
            "kgts,skd->kgtd", grouped, value_heads, preferred_element_type=jnp.float32
        ).reshape(head_count, local_rows, HEAD)
        new_acc = run_acc * factor[:, :, None] + product
        return (new_max, new_sum, new_acc)

    shard_rows = key_rows.shape[0]

    def fold_keys(state, pieces, start):
        key_piece, value_piece = pieces
        span = key_piece.shape[0]
        shards_in = span // shard_rows
        group = 1
        for divisor in range(1, shards_in + 1):
            if shards_in % divisor == 0 and divisor * shard_rows <= 2048:
                group = divisor
        block = group * shard_rows
        if block >= span:
            return attend_block(state, key_piece, value_piece, start)
        key_blocks = key_piece.reshape(span // block, block, kv_cols)
        value_blocks = value_piece.reshape(span // block, block, kv_cols)
        firsts = start + block * jnp.arange(span // block, dtype=jnp.int32)

        def step_block(inner, items):
            return (attend_block(inner, items[0], items[1], items[2]), None)

        result, unused = lax.scan(step_block, state, (key_blocks, value_blocks, firsts))
        return result

    start_state = (
        jnp.full((head_count, local_rows), -1e30, jnp.float32),
        jnp.zeros((head_count, local_rows), jnp.float32),
        jnp.zeros((head_count, local_rows, HEAD), jnp.float32),
    )
    run_max, run_sum, run_acc = fold_keys(
        start_state, sent_together((key_rows, value_rows), "sp", 0, 1), jnp.int32(0)
    )
    attended = jnp.transpose(
        (run_acc / run_sum[:, :, None]).astype(jnp.bfloat16), (1, 0, 2)
    ).reshape(local_rows, query_cols)
    rim = shifted(glu[local_rows - (KW - 1) :], "sp", 1)
    padded = jnp.concatenate([rim, glu], axis=0).astype(jnp.float32)
    taps = conv_taps.astype(jnp.float32)
    conv = jnp.zeros((local_rows, conv_cols), jnp.float32)
    for shift_tap in range(KW):
        conv = conv + taps[shift_tap][None, :] * padded[shift_tap : shift_tap + local_rows]
    first_sum, square_sum = in_one((jnp.sum(conv, axis=1), jnp.sum(conv * conv, axis=1)), "tp")
    mean_c = (first_sum / CONV)[:, None]
    var_c = (square_sum / CONV)[:, None] - mean_c * mean_c
    shaped = (conv - mean_c) * lax.rsqrt(var_c + 1e-05) * conv_gain.astype(
        jnp.float32
    ) + conv_bias.astype(jnp.float32)
    conv_act = jax.nn.silu(shaped).astype(jnp.bfloat16)
    att_weight, conv_weight = gather_turned((w_out_att, w_out_conv), "sp", (1, 1))
    terms = jnp.dot(attended, att_weight, preferred_element_type=jnp.float32) + jnp.dot(
        conv_act, conv_weight, preferred_element_type=jnp.float32
    )
    return sum_at_owner(terms.astype(jnp.bfloat16), "tp", 1).astype(jnp.bfloat16)


def solution(mesh):
    return jax.shard_map(
        shards,
        mesh=mesh,
        in_specs=(
            P(("sp", "tp"), None),
            P(),
            P(None, "tp"),
            P(None, "tp"),
            P(None, "tp"),
            P(None, "tp"),
            P(None, "tp"),
            P(None, "tp"),
            P("tp"),
            P("tp"),
            P(None, "tp"),
            P("tp", "sp"),
            P("tp", "sp"),
        ),
        out_specs=P("sp", "tp"),
        check_vma=False,
    )
```

profile of v0, /device:TPU:1, one launch (start us, length us, event | category | flops | bytes accessed | tf_op | source)
XLA Modules:
  0.0 269.8 jit_solution(8019864860695089635)
XLA Ops:
  8.5 4.8 %all-to-all-start = ((bf16[4,32,2048]{2,1,0:T(8,128)(2,1)}), bf16[4,32,2048]{2,1,0:T(8,128)(2,1)S(1)}, u32[]{:S(2)}, u32[]{:S(2)}) async-start(bf16[4,32,2048]{2,1,0:T(8,128)(2,1)} %broadcast_in_dim.56), calls=%async_computation | async-start | bytes 1048576 | tf_op jit(solution)/shard_map/all_to_all | solution.py:21
  14.0 6.2 %all-to-all-done = bf16[4,32,2048]{2,1,0:T(8,128)(2,1)S(1)} async-done(((bf16[4,32,2048]{2,1,0:T(8,128)(2,1)}), bf16[4,32,2048]{2,1,0:T(8,128)(2,1)S(1)}, u32[]{:S(2)}, u32[]{:S(2)}) %all-to-all-start) | async-done | bytes 524320 | tf_op jit(solution)/shard_map/all_to_all | solution.py:21
  26.0 6.6 %collective-permute-start = (bf16[30,256]{1,0:T(8,128)(2,1)S(1)}, bf16[30,256]{1,0:T(8,128)(2,1)S(1)}, u32[]{:S(2)}, u32[]{:S(2)}) collective-permute-start(bf16[30,256]{1,0:T(8,128)(2,1)S(1)} %slice.270), channel_id=1, source_target_pairs={{0,4},{4,8},{8,12},{12,16},{16,20},{20,24},{24,28},{28,32},{32,36}... | collective-permute-start | bytes 46088 | tf_op jit(solution)/shard_map/ppermute | solution.py:38
  35.8 3.2 %all-to-all-start.1 = ((f32[4,1,256]{2,1,0:T(1,128)}), f32[4,1,256]{2,1,0:T(1,128)S(1)}, u32[]{:S(2)}, u32[]{:S(2)}) async-start(f32[4,1,256]{2,1,0:T(1,128)} %broadcast_in_dim.57), calls=%async_computation.1 | async-start | bytes 8192 | tf_op jit(solution)/shard_map/all_to_all | solution.py:21
  40.0 3.1 %all-to-all-done.1 = f32[4,1,256]{2,1,0:T(1,128)S(1)} async-done(((f32[4,1,256]{2,1,0:T(1,128)}), f32[4,1,256]{2,1,0:T(1,128)S(1)}, u32[]{:S(2)}, u32[]{:S(2)}) %all-to-all-start.1) | async-done | bytes 4128 | tf_op jit(solution)/shard_map/all_to_all | solution.py:21
  43.8 78.0 %all-gather.3.cloned.1.call-done = bf16[16384,256]{0,1:T(8,128)(2,1)} async-done(((bf16[128,256]{0,1:T(8,128)(2,1)}), bf16[16384,256]{0,1:T(8,128)(2,1)}) %all-gather.3.cloned.1.call-update) | async-done | bytes 8388624 | tf_op jit(solution)/shard_map/all_gather | solution.py:31
  121.7 5.8 %fusion.79 = (bf16[16384,128]{0,1:T(8,128)(2,1)}, bf16[16384,128]{0,1:T(8,128)(2,1)}) fusion(bf16[16384,256]{0,1:T(8,128)(2,1)} %all-gather.3.cloned.1.call-done), kind=kLoop, calls=%fused_computation.140 | loop fusion | bytes 16777216 | tf_op jit(solution)/shard_map/split | solution.py:32
  127.6 6.4 %copy.43 = bf16[16384,128]{1,0:T(8,128)(2,1)} copy(bf16[16384,128]{0,1:T(8,128)(2,1)} %get-tuple-element.189) | data formatting | bytes 8388608
  133.9 6.4 %copy.44 = bf16[16384,128]{1,0:T(8,128)(2,1)} copy(bf16[16384,128]{0,1:T(8,128)(2,1)} %get-tuple-element.188) | data formatting | bytes 8388608
  140.4 104.8 %while.15 = (s32[]{:T(128)}, f32[2,128]{1,0:T(2,128)}, f32[2,128]{1,0:T(2,128)}, f32[2,128,128]{2,1,0:T(8,128)}, s32[8]{0:T(128)}, /*index=5*/bf16[8,2048,128]{2...) while((s32[]{:T(128)}, f32[2,128]{1,0:T(2,128)}, ...), condition=%wide.region_4.5_spmd.clone, body=%wide.region_1.4_spmd.clone.sunk | while | flops 277712256 | bytes 9901427 | solution.py:167
  144.9 2.3 fusion.101
  149.9 2.3 convolution_add_fusion.3
  158.0 2.3 fusion.101
  171.1 2.3 fusion.101
  176.1 2.3 convolution_add_fusion.3
  184.2 2.3 fusion.101
  189.2 2.3 convolution_add_fusion.3
  197.2 2.3 fusion.101
  202.3 2.3 convolution_add_fusion.3
  210.4 2.3 fusion.101
  223.5 2.3 fusion.101
  236.6 2.3 fusion.101
  241.6 2.3 convolution_add_fusion.3
  249.3 12.8 %all_to_all.16 = bf16[4,128,512]{2,1,0:T(8,128)(2,1)S(1)} all-to-all(bf16[4,128,512]{2,1,0:T(8,128)(2,1)S(1)} %bitcast.135), channel_id=1, replica_groups=mesh['sp'=128,'tp'=4] {'tp'}, dimensions={0} | all-to-all | bytes 1048576 | tf_op jit(solution)/shard_map/all_to_all | solution.py:72
  (242 shorter events, 78.7 us)
Async XLA Ops:
  6.5 17.6 %copy-start = (bf16[2048,256]{1,0:T(8,128)(2,1)S(1)}, bf16[2048,256]{1,0:T(8,128)(2,1)}, u32[]{:S(2)}) copy-start(bf16[2048,256]{1,0:T(8,128)(2,1)} %param.20) | copy-start | bytes 3145732
  6.5 14.2 %copy-start.3 = (bf16[2048,128]{1,0:T(8,128)(2,1)S(1)}, bf16[2048,128]{1,0:T(8,128)(2,1)}, u32[]{:S(2)}) copy-start(bf16[2048,128]{1,0:T(8,128)(2,1)} %param.19) | copy-start | bytes 1572868
  6.5 14.5 %copy-start.4 = (bf16[2048,128]{1,0:T(8,128)(2,1)S(1)}, bf16[2048,128]{1,0:T(8,128)(2,1)}, u32[]{:S(2)}) copy-start(bf16[2048,128]{1,0:T(8,128)(2,1)} %param.18) | copy-start | bytes 1572868
  8.5 11.8 %all-to-all-start = ((bf16[4,32,2048]{2,1,0:T(8,128)(2,1)}), bf16[4,32,2048]{2,1,0:T(8,128)(2,1)S(1)}, u32[]{:S(2)}, u32[]{:S(2)}) async-start(bf16[4,32,2048]{2,1,0:T(8,128)(2,1)} %broadcast_in_dim.56), calls=%async_computation | async-start | bytes 1048576 | tf_op jit(solution)/shard_map/all_to_all | solution.py:21
  13.3 8.9 %copy-start.12 = (bf16[256,16]{0,1:T(8,128)(2,1)S(1)}, bf16[256,16]{0,1:T(8,128)(2,1)}, u32[]{:S(2)}) copy-start(bf16[256,16]{0,1:T(8,128)(2,1)} %param.27) | copy-start | bytes 24580
  13.3 8.9 %copy-start.13 = (bf16[256,16]{0,1:T(8,128)(2,1)S(1)}, bf16[256,16]{0,1:T(8,128)(2,1)}, u32[]{:S(2)}) copy-start(bf16[256,16]{0,1:T(8,128)(2,1)} %param.26) | copy-start | bytes 24580
  13.3 9.6 %copy-start.8 = (bf16[31,256]{1,0:T(8,128)(2,1)S(1)}, bf16[31,256]{1,0:T(8,128)(2,1)}, u32[]{:S(2)}) copy-start(bf16[31,256]{1,0:T(8,128)(2,1)} %param.22) | copy-start | bytes 47620
  13.3 108.4 %all-gather.3.cloned.1.call-start = ((), (), s32[]{:S(2)}) async-start(), calls=%async_computation.3 | async-start | bytes 8454144 | tf_op jit(solution)/shard_map/all_gather | solution.py:31
  21.4 11.7 %copy-start.18 = (bf16[256]{0:T(256)(128)(2,1)S(1)}, bf16[256]{0:T(256)(128)(2,1)}, u32[]{:S(2)}) copy-start(bf16[256]{0:T(256)(128)(2,1)} %param.23) | copy-start | bytes 1540
  21.4 12.3 %copy-start.19 = (bf16[256]{0:T(256)(128)(2,1)S(1)}, bf16[256]{0:T(256)(128)(2,1)}, u32[]{:S(2)}) copy-start(bf16[256]{0:T(256)(128)(2,1)} %param.24) | copy-start | bytes 1540
  22.1 224.8 %all-gather.5.cloned.1.call-start = ((), (), s32[]{:S(2)}) async-start(), calls=%async_computation.4 | async-start | bytes 2113536 | tf_op jit(solution)/shard_map/all_gather | solution.py:57
  26.0 8.5 %collective-permute-start = (bf16[30,256]{1,0:T(8,128)(2,1)S(1)}, bf16[30,256]{1,0:T(8,128)(2,1)S(1)}, u32[]{:S(2)}, u32[]{:S(2)}) collective-permute-start(bf16[30,256]{1,0:T(8,128)(2,1)S(1)} %slice.270), channel_id=1, source_target_pairs={{0,4},{4,8},{8,12},{12,16},{16,20},{20,24},{24,28},{28,32},{32,36}... | collective-permute-start | bytes 46088 | tf_op jit(solution)/shard_map/ppermute | solution.py:38
  34.6 4.4 %copy-start.2 = (bf16[2048,256]{1,0:T(8,128)(2,1)S(1)}, bf16[2048,256]{1,0:T(8,128)(2,1)}, u32[]{:S(2)}) copy-start(bf16[2048,256]{1,0:T(8,128)(2,1)} %param.17) | copy-start | bytes 3145732
  35.8 7.3 %all-to-all-start.1 = ((f32[4,1,256]{2,1,0:T(1,128)}), f32[4,1,256]{2,1,0:T(1,128)S(1)}, u32[]{:S(2)}, u32[]{:S(2)}) async-start(f32[4,1,256]{2,1,0:T(1,128)} %broadcast_in_dim.57), calls=%async_computation.1 | async-start | bytes 8192 | tf_op jit(solution)/shard_map/all_to_all | solution.py:21
  160.3 2.7 %copy-start.9 = (f32[2,128]{1,0:T(2,128)S(1)}, f32[2,128]{1,0:T(2,128)}, u32[]{:S(2)}) copy-start(f32[2,128]{1,0:T(2,128)} %get-tuple-element.333) | copy-start | bytes 3076 | tf_op jit(solution)/shard_map/while
  173.4 2.7 %copy-start.9 = (f32[2,128]{1,0:T(2,128)S(1)}, f32[2,128]{1,0:T(2,128)}, u32[]{:S(2)}) copy-start(f32[2,128]{1,0:T(2,128)} %get-tuple-element.333) | copy-start | bytes 3076 | tf_op jit(solution)/shard_map/while
  186.5 2.7 %copy-start.9 = (f32[2,128]{1,0:T(2,128)S(1)}, f32[2,128]{1,0:T(2,128)}, u32[]{:S(2)}) copy-start(f32[2,128]{1,0:T(2,128)} %get-tuple-element.333) | copy-start | bytes 3076 | tf_op jit(solution)/shard_map/while
  199.6 2.7 %copy-start.9 = (f32[2,128]{1,0:T(2,128)S(1)}, f32[2,128]{1,0:T(2,128)}, u32[]{:S(2)}) copy-start(f32[2,128]{1,0:T(2,128)} %get-tuple-element.333) | copy-start | bytes 3076 | tf_op jit(solution)/shard_map/while
  212.7 2.7 %copy-start.9 = (f32[2,128]{1,0:T(2,128)S(1)}, f32[2,128]{1,0:T(2,128)}, u32[]{:S(2)}) copy-start(f32[2,128]{1,0:T(2,128)} %get-tuple-element.333) | copy-start | bytes 3076 | tf_op jit(solution)/shard_map/while
  238.9 2.7 %copy-start.9 = (f32[2,128]{1,0:T(2,128)S(1)}, f32[2,128]{1,0:T(2,128)}, u32[]{:S(2)}) copy-start(f32[2,128]{1,0:T(2,128)} %get-tuple-element.333) | copy-start | bytes 3076 | tf_op jit(solution)/shard_map/while
  245.1 3.6 %copy-start.14 = (f32[128]{0:T(128)S(1)}, f32[128]{0:T(128)}, u32[]{:S(2)}) copy-start(f32[128]{0:T(128)} %get-tuple-element.221) | copy-start | bytes 1540
  245.1 3.6 %copy-start.15 = (f32[128]{0:T(128)S(1)}, f32[128]{0:T(128)}, u32[]{:S(2)}) copy-start(f32[128]{0:T(128)} %get-tuple-element.222) | copy-start | bytes 1540
  245.1 3.6 %copy-start.16 = (f32[256]{0:T(256)S(1)}, f32[256]{0:T(256)}, u32[]{:S(2)}) copy-start(f32[256]{0:T(256)} %convert_element_type.66) | copy-start | bytes 3076
  245.1 3.6 %copy-start.17 = (f32[256]{0:T(256)S(1)}, f32[256]{0:T(256)}, u32[]{:S(2)}) copy-start(f32[256]{0:T(256)} %convert_element_type.67) | copy-start | bytes 3076
  (43 other events, 72.6 us)
Sparse Core Ops, SparseCore 0:
  22.2 99.4 all-gather.2
  124.9 78.5 all-gather.4
where the time goes:
time: 272 us; the launch traced here: 270 us
  waiting for transfers between devices  87.6 us (32%)
  local copies, waits for them, and re-layouts  54.1 us (20%)
  matrix products  42.4 us (16%)
  other arithmetic  30.6 us (11%)
  starting transfers between devices  14.7 us (5%)
  loops' own time  13.8 us (5%)
  between operations  13.7 us (5%)
  blocking collectives  12.8 us (5%)
    all_gather x1, waiting for transfers between devices, sent_together(): out = lax.all_gather(both, axis, axis=dim, tiled=True)  78 us
    dot_general x8, matrix products, attend_block(): jnp.einsum('tkgd,skd->kgts', query_groups, key_heads, preferred_element_t...  18.7 us
    dot_general x8, matrix products, attend_block(): jnp.einsum('kgts,skd->kgtd', grouped, value_heads, preferred_element_type...  18.4 us
    while x104, local copies, waits for them, and re-layouts  14.2 us
    another operation x1, loops' own time, fold_keys(): lax.scan(step_block, state, (key_blocks, value_blocks, firsts))  13.8 us
    unnamed x31, local copies, waits for them, and re-layouts  13.5 us
    all_to_all x1, blocking collectives, sum_at_owner(): lax.all_to_all(blocks, axis, split_axis=0, concat_axis=0, tiled=True)  12.8 us
    reduce_sum x8, other arithmetic, attend_block(): new_sum = run_sum * factor + jnp.sum(weights, axis=-1)  11.1 us
  transfers between devices with their start and end apart: 5, of which 4 were waited for; matrix products, arithmetic and copies ran while one was open for 41% of the time, Pallas kernels for 0%

commit v1 on v0

v1 whole, which is shorter than its diff:
```python
import math

import jax
import jax.numpy as jnp
from jax import lax
from jax.experimental import pallas as pl
from jax.experimental.pallas import tpu as pltpu
from jax.sharding import PartitionSpec as P

HEAD = 128
KW = 31
ROWS = 128
LOG2E = math.log2(math.e)
FAR = 1e30
MESH = pl.DeviceIdType.MESH
F32 = jnp.float32
BF16 = jnp.bfloat16


def nt(a, b):
    return lax.dot_general(a, b, (((1,), (1,)), ((), ())), preferred_element_type=F32)


def nn(a, b):
    return lax.dot_general(a, b, (((1,), (0,)), ((), ())), preferred_element_type=F32)


class Sems:
    def __init__(self, send, recv):
        self.send, self.recv, self.used = send, recv, 0

    def take(self, count=1):
        first = self.used
        self.used += count
        return first


class Ring:
    def __init__(self, n, sems, chunks, plus, minus, here, there):
        self.n, self.chunks, self.here, self.there = n, chunks, here, there
        self.peer = {1: plus, -1: minus}
        self.hops = {1: n // 2, -1: (n - 1) // 2}
        self.base = sems.take((n - 1) * chunks) if n > 1 else 0
        self.sems = sems
        self.started = []

    def index(self, way, k, ch):
        return self.base + ((k - 1) if way > 0 else self.hops[1] + k - 1) * self.chunks + ch

    def rel(self, way, k):
        return k if way > 0 else (self.n - k) % self.n

    def copy(self, way, k, ch):
        i = self.index(way, k, ch)
        a, b = self.rel(way, k - 1), self.rel(way, k)
        return pltpu.make_async_remote_copy(
            src_ref=self.here(a, ch),
            dst_ref=self.there(a, b, ch),
            send_sem=self.sems.send.at[i],
            recv_sem=self.sems.recv.at[i],
            device_id=self.peer[way],
            device_id_type=MESH,
        )

    def start(self, way, k, ch):
        if k <= self.hops[way]:
            c = self.copy(way, k, ch)
            c.start()
            self.started.append(c)

    def arrive(self, way, k, ch):
        i = self.index(way, k, ch)
        slot = self.here(self.rel(way, k), ch)
        pltpu.make_async_remote_copy(
            src_ref=slot,
            dst_ref=slot,
            send_sem=self.sems.send.at[i],
            recv_sem=self.sems.recv.at[i],
            device_id=self.peer[-way],
            device_id_type=MESH,
        ).wait_recv()

    def step(self, way, k, after=None):
        if k > self.hops[way]:
            return
        for ch in range(self.chunks):
            self.arrive(way, k, ch)
            self.start(way, k + 1, ch)
            if after is not None:
                after(self.rel(way, k), ch)


def layer_kernel(
    nz, ny, nx,
    tokens, gain, wq, wk, wv, wcv, wcg, taps, cgain, cbias, gate, wa_t, wc_t,
    out,
    tok_all, wbuf, qsend, qbuf, kv, conv_in, halo_out, halo_in, conv_s, st_out, st_in,
    wt, s_ref, gkb, o_out, o_in, rs_out, rs_in, proj_s, wsem, send, recv,
):
    rows = ROWS
    chip = 2 * rows
    dim = tokens.shape[1]
    trows = tokens.shape[0]
    chans = wcv.shape[1]
    ocols = out.shape[1]
    sp = lax.axis_index("sp")
    x = lax.axis_index("tp")
    c = lax.rem(sp, 2)
    y = lax.rem(lax.div(sp, 2), ny)
    z = lax.div(sp, 2 * ny)
    nsp = nz * ny * 2

    def at(zz, yy, cc):
        return (zz * ny + yy) * 2 + cc

    def mod(a, n):
        return lax.rem(a + 2 * n, n)

    sems = Sems(send, recv)
    pending = []

    def remote(src, dst, i, dev, ri=None):
        return pltpu.make_async_remote_copy(
            src_ref=src,
            dst_ref=dst,
            send_sem=send.at[i],
            recv_sem=recv.at[i if ri is None else ri],
            device_id=dev,
            device_id_type=MESH,
        )

    def launch(src, dst, i, dev, ri=None):
        cp = remote(src, dst, i, dev, ri)
        cp.start()
        pending.append(cp)

    sib = (at(z, y, 1 - c), x)

    wcols, off = [], 0
    for k, w in enumerate((wq, wk, wv, wcv, wcg)):
        cp = pltpu.make_async_copy(w, wbuf.at[:, off : off + w.shape[1]], wsem.at[k])
        cp.start()
        wcols.append(cp)
        off += w.shape[1]

    barrier = pltpu.get_barrier_semaphore()
    peers = [(sp, mod(x + d, nx)) for d in range(1, nx)]
    peers += [(at(z, mod(y + d, ny), cc), x) for d in range(1, ny) for cc in range(2)]
    peers += [sib]
    if nz > 1:
        peers += [(at(mod(z + d, nz), y, c), x) for d in (1, -1)]
    nxt, prv = mod(sp + 1, nsp), mod(sp - 1, nsp)
    peers += [(nxt, x), (prv, x)]
    for p in peers:
        pl.semaphore_signal(barrier, inc=1, device_id=p, device_id_type=MESH)

    tok = tokens[...].astype(F32)
    mean_sq = jnp.mean(tok * tok, axis=-1, keepdims=True)
    tok_all[x] = (tok * lax.rsqrt(mean_sq + 1e-06) * gain[...].astype(F32)).astype(BF16)
    wt[z, y, c, :, :256] = wa_t[...]
    wt[z, y, c, :, 256:] = wc_t[...]

    pl.semaphore_wait(barrier, len(peers))

    tok_i = sems.take(nx)
    order = sorted(range(1, nx), key=lambda d: -min(d, nx - d))
    for d in order:
        launch(tok_all.at[x], tok_all.at[x], tok_i + d, (sp, mod(x + d, nx)))

    wy = Ring(
        ny, sems, 1,
        (at(z, mod(y + 1, ny), c), x), (at(z, mod(y - 1, ny), c), x),
        lambda r, ch: wt.at[z, mod(y - r, ny), c],
        lambda a, b, ch: wt.at[z, mod(y - a, ny), c],
    )
    wz = Ring(
        nz, sems, 1,
        (at(mod(z + 1, nz), y, c), x), (at(mod(z - 1, nz), y, c), x),
        lambda r, ch: wt.at[mod(z - r, nz), :, c],
        lambda a, b, ch: wt.at[mod(z - a, nz), :, c],
    )
    qr = Ring(
        ny, sems, 2,
        (at(z, mod(y + 1, ny), c), x), (at(z, mod(y - 1, ny), c), x),
        lambda r, ch: qbuf.at[r, pl.ds(pl.multiple_of((c if ch == 0 else 1 - c) * rows, rows), rows)],
        lambda a, b, ch: qbuf.at[b, pl.ds(pl.multiple_of((c if ch == 0 else 1 - c) * rows, rows), rows)],
    )
    kr = Ring(
        nz, sems, 1,
        (at(mod(z + 1, nz), y, c), x), (at(mod(z - 1, nz), y, c), x),
        lambda r, ch: kv.at[r, 0],
        lambda a, b, ch: kv.at[b, 0],
    )
    for way in (1, -1):
        wy.start(way, 1, 0)

    g_first = gate[:, pl.ds(pl.multiple_of(z * ny * chip, chip), 128)]
    g_ref = jnp.where(c == 0, g_first[0:1, 0:1], g_first[1:2, 0:1])

    def gate_row(start, width):
        g = gate[:, pl.ds(pl.multiple_of(start, 128), width)]
        return (jnp.where(c == 0, g[0:1], g[1:2]) - g_ref) * LOG2E

    for s in range(nz):
        for p in range(2):
            cc = c if p == 0 else 1 - c
            g = gate_row(at(mod(z - s, nz), y, cc) * rows, rows)
            g = jnp.where(s <= z, g, FAR)
            gkb[pl.ds((s * 2 + p) * rows, rows), :] = jnp.transpose(jnp.broadcast_to(g, (128, rows)))

    for way in (1, -1):
        wy.step(way, 1)
        wy.step(way, 2)

    for cp in wcols[:3]:
        cp.wait()
    for d in range(1, nx):
        src = mod(x - d, nx)
        remote(tok_all.at[src], tok_all.at[src], tok_i + d, (sp, src)).wait_recv()
    normed = tok_all[...].reshape(rows, dim)
    qw, kw_ = wq.shape[1], wk.shape[1]
    qkv = nn(normed, wbuf[:, : qw + 2 * kw_])
    q0 = qkv[:, :HEAD].astype(BF16)
    q1 = qkv[:, HEAD:qw].astype(BF16)
    kv[0, 0, :rows] = qkv[:, qw : qw + kw_].astype(BF16)
    kv[0, 0, rows:] = jnp.transpose(qkv[:, qw + kw_ :]).astype(BF16)
    mine = pl.ds(pl.multiple_of(c * rows, rows), rows)
    qbuf[0, mine] = jnp.where(c == 0, q0, q1)
    qsend[...] = jnp.where(c == 0, q1, q0)

    q_i = sems.take()
    launch(qsend, qbuf.at[0, mine], q_i, sib)
    for way in (1, -1):
        qr.start(way, 1, 0)
        kr.start(way, 1, 0)
    ks_i = sems.take(nz)

    def pass_kv(rel, ch):
        launch(kv.at[rel, 0], kv.at[rel, 1], ks_i + rel, sib)

    pass_kv(0, 0)
    theirs = pl.ds(pl.multiple_of((1 - c) * rows, rows), rows)
    remote(qsend, qbuf.at[0, theirs], q_i, sib).wait_recv()
    for way in (1, -1):
        qr.start(way, 1, 1)

    for cp in wcols[3:]:
        cp.wait()
    halves = nn(normed, wbuf[:, qw + 2 * kw_ :])
    glu = (halves[:, :chans] * jax.nn.sigmoid(halves[:, chans:])).astype(BF16)
    conv_in[32:] = glu.astype(F32)
    halo_out[...] = glu[rows - 32 :]
    h_i = sems.take()
    launch(halo_out, halo_in, h_i, (nxt, x))

    for way in (1, -1):
        wy.step(way, 3)
        qr.step(way, 1)
        kr.step(way, 1, pass_kv)

    remote(halo_out, halo_in, h_i, (prv, x)).wait_recv()
    conv_in[:32] = jnp.where(sp == 0, 0.0, halo_in[...].astype(F32))

    for way in (1, -1):
        wy.step(way, 4)
        qr.step(way, 2)
        kr.step(way, 2, pass_kv)

    tap = taps[...].astype(F32)
    half = KW // 2
    conv = jnp.zeros((rows, chans), F32)
    for k in range(half):
        conv = conv + tap[k : k + 1] * conv_in[2 + k : 2 + k + rows]
    for way in (1, -1):
        qr.step(way, 3)
        kr.step(way, 3, pass_kv)
    for k in range(half, KW):
        conv = conv + tap[k : k + 1] * conv_in[2 + k : 2 + k + rows]
    conv_s[...] = conv
    s1 = jnp.sum(conv, axis=1, keepdims=True)
    s2 = jnp.sum(conv * conv, axis=1, keepdims=True)
    lane = lax.broadcasted_iota(jnp.int32, (rows, 128), 1)
    st_out[...] = jnp.transpose(jnp.where(lane == 0, s1, s2))[:8]
    st_i = sems.take(nx)
    for d in order:
        launch(st_out, st_in.at[nx - d], st_i + d, (sp, mod(x + d, nx)))
    for k in range(4, max([0] + [r.hops[1] for r in (qr, kr)]) + 1):
        for way in (1, -1):
            qr.step(way, k)
            kr.step(way, k, pass_kv)
    for way in (1, -1):
        wz.start(way, 1, 0)
    for s in range(nz):
        remote(kv.at[s, 0], kv.at[s, 1], ks_i + s, sib).wait_recv()

    scale = LOG2E / math.sqrt(HEAD)
    ones = jnp.ones((16, chip), BF16)
    o_i = sems.take(ny * 2)
    sub = lax.broadcasted_iota(jnp.int32, (16, rows), 0)
    key_lo = lax.broadcasted_iota(jnp.int32, (rows, chip), 0)
    q_at = lax.broadcasted_iota(jnp.int32, (rows, chip), 1)

    def attend(r):
        jq = mod(y - r, ny)
        qb = qbuf[r]
        peak = jnp.full((8, chip), -FAR, F32)
        for s in range(nz):
            for p in range(2):
                keys = kv[s, p, :rows]
                g = gkb[pl.ds((s * 2 + p) * rows, rows), :]
                t = nt(keys, qb) * scale - jnp.concatenate([g, g], axis=1)
                if s == 0:
                    cc = c if p == 0 else 1 - c
                    shift = (y - jq) * chip + cc * rows
                    t = jnp.where(key_lo + shift <= q_at, t, -FAR)
                s_ref[pl.ds((s * 2 + p) * rows, rows), :] = t
                peak = jnp.maximum(peak, jnp.max(t.reshape(rows // 8, 8, chip), axis=0))
        m = jnp.max(peak, axis=0, keepdims=True)
        acc = jnp.zeros((HEAD + 16, chip), F32)
        for s in range(nz):
            w = jnp.exp2(s_ref[pl.ds(s * chip, chip), :] - m).astype(BF16)
            vt = jnp.concatenate([kv[s, 0, rows:], kv[s, 1, rows:]], axis=1)
            acc = acc + nn(jnp.concatenate([vt, ones], axis=0), w)
        den = acc[HEAD : HEAD + 1]
        o = (acc[:HEAD] / den).astype(BF16)
        m = m + gate_row((z * ny + jq) * chip, chip)
        m1 = m.astype(BF16).astype(F32)
        m2 = (m - m1).astype(BF16).astype(F32)
        d1 = den.astype(BF16).astype(F32)
        d2 = (den - d1).astype(BF16).astype(F32)
        parts = (m1, m2, m - m1 - m2, d1, d2, den - d1 - d2)
        for cc in range(2):
            lanes = slice(cc * rows, (cc + 1) * rows)
            tile = jnp.zeros((16, rows), F32)
            for i, part in enumerate(parts):
                tile = jnp.where(sub == i, part[:, lanes], tile)
            o_out[r, cc, :HEAD] = o[:, lanes]
            o_out[r, cc, HEAD:] = tile.astype(BF16)

    ring_order = sorted(range(ny), key=lambda r: (-min(r, ny - r), r))
    for n, r in enumerate(ring_order):
        attend(r)
        if r:
            for cc in range(2):
                launch(o_out.at[r, cc], o_in.at[r, c], o_i + 2 * r + cc, (at(z, mod(y - r, ny), cc), x), o_i + 2 * r + c)
        if n % 2 == 1 and n // 2 + 1 <= nz // 2:
            for way in (1, -1):
                wz.step(way, n // 2 + 1)
    for k in range(ny // 2 + 1, nz // 2 + 1):
        for way in (1, -1):
            wz.step(way, k)
    launch(o_out.at[0, 1 - c], o_in.at[0, c], o_i + 1 - c, sib, o_i + c)

    ws_i = sems.take(nz)
    for s in range(nz):
        zz = mod(z - s, nz)
        launch(wt.at[zz, :, c], wt.at[zz, :, c], ws_i + s, sib)

    tot = st_out[...]
    for d in range(1, nx):
        remote(st_out, st_in.at[nx - d], st_i + d, (sp, mod(x - d, nx))).wait_recv()
        tot = tot + st_in[nx - d]
    total_chans = chans * nx
    mean_r = tot[0:1] / total_chans
    var_r = tot[1:2] / total_chans - mean_r * mean_r
    rstd_r = lax.rsqrt(var_r + 1e-05)
    mean_c = jnp.transpose(jnp.broadcast_to(mean_r, (128, rows)))
    rstd_c = jnp.transpose(jnp.broadcast_to(rstd_r, (128, rows)))
    wide = chans // 128
    mean_c = jnp.concatenate([mean_c] * wide, axis=1)
    rstd_c = jnp.concatenate([rstd_c] * wide, axis=1)
    shaped = (conv_s[...] - mean_c) * rstd_c * cgain[...].astype(F32) + cbias[...].astype(F32)
    conv_act = (shaped / (1.0 + jnp.exp(-shaped))).astype(BF16)

    for s in range(nz):
        zz = mod(z - s, nz)
        remote(wt.at[zz, :, 1 - c], wt.at[zz, :, 1 - c], ws_i + s, sib).wait_recv()
    per = nz // nx
    for d in range(nx):
        xx = mod(x + d, nx)
        w = wt[pl.ds(xx * per, per), :, :, :, 256:].reshape(ocols, chans)
        proj_s[d] = nt(conv_act, w)

    o_in[0, c] = o_out[0, c]
    for r in range(ny):
        for hh in range(2):
            if r:
                slot, frm = o_in.at[r, hh], (at(z, mod(y + r, ny), hh), x)
                remote(slot, slot, o_i + 2 * r + hh, frm).wait_recv()
    slot = o_in.at[0, 1 - c]
    remote(slot, slot, o_i + 1 - c, sib).wait_recv()
    heads = []
    for hh in range(2):
        tiles = [o_in[r, hh, HEAD:].astype(F32) for r in range(ny)]
        tops = [t[0:1] + t[1:2] + t[2:3] for t in tiles]
        dens = [t[3:4] + t[4:5] + t[5:6] for t in tiles]
        top = tops[0]
        for t in tops[1:]:
            top = jnp.maximum(top, t)
        scaled = [d * jnp.exp2(t - top) for d, t in zip(dens, tops)]
        den = scaled[0]
        for d in scaled[1:]:
            den = den + d
        acc = jnp.zeros((HEAD, rows), F32)
        for r in range(ny):
            acc = acc + o_in[r, hh, :HEAD].astype(F32) * (scaled[r] / den)
        heads.append(jnp.transpose(acc).astype(BF16))
    attended = jnp.concatenate(heads, axis=1)

    rs_i = sems.take(nx)
    for d in order + [0]:
        xx = mod(x + d, nx)
        w = wt[pl.ds(xx * per, per), :, :, :, :256].reshape(ocols, 256)
        part = proj_s[d] + nt(attended, w)
        if d:
            rs_out[d] = part.astype(BF16)
            launch(rs_out.at[d], rs_in.at[d], rs_i + d, (sp, xx))
        else:
            total = part
    for d in range(1, nx):
        remote(rs_in.at[d], rs_in.at[d], rs_i + d, (sp, mod(x - d, nx))).wait_recv()
        total = total + rs_in[d].astype(F32)
    out[...] = total.astype(BF16)

    for cp in pending:
        cp.wait_send()
    for ring in (wy, wz, qr, kr):
        for cp in ring.started:
            cp.wait_send()


def layer(nz, ny, nx, *args):
    (tokens, gain, wq, wk, wv, wcv, wcg, taps, cgain, cbias, cum_gate, wa, wc) = args
    dim = tokens.shape[1]
    trows = tokens.shape[0]
    rows, chip = ROWS, 2 * ROWS
    nsp = nz * ny * 2
    chans = wcv.shape[1]
    wcol = wa.shape[1]
    cols = wq.shape[1] + wk.shape[1] + wv.shape[1] + wcv.shape[1] + wcg.shape[1]
    ocols = wcol * nsp // nx
    vm = pl.BlockSpec(memory_space=pltpu.VMEM)
    hb = pl.BlockSpec(memory_space=pl.ANY)
    nsem = nx * 3 + (ny - 1) * 3 + (nz - 1) * 2 + 2 * nz + 2 * ny + 4
    scratch = [
        pltpu.VMEM((nx, trows, dim), BF16),
        pltpu.VMEM((dim, cols), BF16),
        pltpu.VMEM((rows, HEAD), BF16),
        pltpu.VMEM((ny, chip, HEAD), BF16),
        pltpu.VMEM((nz, 2, rows + HEAD, 128), BF16),
        pltpu.VMEM((32 + rows, chans), F32),
        pltpu.VMEM((32, chans), BF16),
        pltpu.VMEM((32, chans), BF16),
        pltpu.VMEM((rows, chans), F32),
        pltpu.VMEM((8, 128), F32),
        pltpu.VMEM((nx, 8, 128), F32),
        pltpu.VMEM((nz, ny, 2, wcol, 512), BF16),
        pltpu.VMEM((nz * chip, chip), F32),
        pltpu.VMEM((nz * chip, 128), F32),
        pltpu.VMEM((ny, 2, HEAD + 16, rows), BF16),
        pltpu.VMEM((ny, 2, HEAD + 16, rows), BF16),
        pltpu.VMEM((nx, rows, ocols), BF16),
        pltpu.VMEM((nx, rows, ocols), BF16),
        pltpu.VMEM((nx, rows, ocols), F32),
        pltpu.SemaphoreType.DMA((5,)),
        pltpu.SemaphoreType.DMA((nsem,)),
        pltpu.SemaphoreType.DMA((nsem,)),
    ]

    def kernel(*refs):
        layer_kernel(nz, ny, nx, *refs)

    return pl.pallas_call(
        kernel,
        out_shape=jax.ShapeDtypeStruct((rows, ocols), BF16),
        in_specs=[vm, vm, hb, hb, hb, hb, hb, vm, vm, vm, vm, vm, vm],
        out_specs=vm,
        scratch_shapes=scratch,
        compiler_params=pltpu.CompilerParams(
            collective_id=0, has_side_effects=True, vmem_limit_bytes=48 * 1024 * 1024
        ),
        name="layer",
    )(
        tokens, gain.reshape(1, dim), wq, wk, wv, wcv, wcg, taps, cgain.reshape(1, chans), cbias.reshape(1, chans),
        cum_gate.T, wa.T, wc.T,
    )


def build(mesh, nz, ny):
    nx = mesh.shape["tp"]

    def shards(*args):
        return layer(nz, ny, nx, *args)

    return jax.shard_map(
        shards,
        mesh=mesh,
        in_specs=(
            P(("sp", "tp"), None),
            P(),
            P(None, "tp"),
            P(None, "tp"),
            P(None, "tp"),
            P(None, "tp"),
            P(None, "tp"),
            P(None, "tp"),
            P("tp"),
            P("tp"),
            P(None, "tp"),
            P("tp", "sp"),
            P("tp", "sp"),
        ),
        out_specs=P("sp", "tp"),
        check_vma=False,
    )


def solution(mesh):
    side = math.isqrt(mesh.shape["sp"] // 2)
    return build(mesh, side, side)
```

time: 272 us -> 81.2 us (0.30)
  waiting for transfers between devices: 87.6 us -> 0 us
  Pallas kernels: 0 us -> 69 us
  local copies, waits for them, and re-layouts: 54.1 us -> 11.6 us
  matrix products: 42.4 us -> 0 us
  other arithmetic: 30.6 us -> 0 us
  starting transfers between devices: 14.7 us -> 0 us
  loops' own time: 13.8 us -> 0 us
  between operations: 13.7 us -> 0.03 us
  blocking collectives: 12.8 us -> 0 us
    all_gather x2 -> x0, waiting for transfers between devices: 78 us -> none  [the longest x1 78 us: sent_together(): out = lax.all_gather(both, axis, axis=dim, tiled=True)]
    pallas_call x0 -> x1, Pallas kernels: none -> 69 us  [layer(): pl.pallas_call(kernel, out_shape=jax.ShapeDtypeStruct((rows, ocols), BF16...]
    dot_general x23 -> x0, matrix products: 42.4 us -> none  [the longest x8 18.7 us: attend_block(): jnp.einsum('tkgd,skd->kgts', query_groups, key_heads, preferred_element_t...]
    while x105 -> x0, local copies, waits for them, and re-layouts: 15.2 us -> none
    another operation x1 -> x0, loops' own time: 13.8 us -> none  [fold_keys(): lax.scan(step_block, state, (key_blocks, value_blocks, firsts))]
    all_to_all x1 -> x0, blocking collectives: 12.8 us -> none  [sum_at_owner(): lax.all_to_all(blocks, axis, split_axis=0, concat_axis=0, tiled=True)]
    reduce_sum x12 -> x0, other arithmetic: 12.7 us -> none  [the longest x8 11.1 us: attend_block(): new_sum = run_sum * factor + jnp.sum(weights, axis=-1)]
    all_to_all x2 -> x0, waiting for transfers between devices: 9.31 us -> none  [sent_to_all(): return lax.all_to_all(copies, axis, split_axis=0, concat_axis=0, tiled=True)]
  transfers between devices with their start and end apart: 5 -> 0, of which waited for: 4 -> 0; matrix products, arithmetic and copies ran while one was open for 41% -> 0% of each run, Pallas kernels for 0% -> 0%
where the time goes in v1:
time: 81.2 us; the launch traced here: 80.6 us
  Pallas kernels  69 us (85%)
  local copies, waits for them, and re-layouts  11.6 us (14%)
    pallas_call x1, Pallas kernels, layer(): pl.pallas_call(kernel, out_shape=jax.ShapeDtypeStruct((rows, ocols), BF16...  69 us
    unnamed x21, local copies, waits for them, and re-layouts  9.61 us

profile of v1, /device:TPU:1, one launch (start us, length us, event | category | flops | bytes accessed | tf_op | source)
XLA Modules:
  0.0 80.6 jit_solution(13611017628147988320)
XLA Ops:
  0.0 0.0 copy-start.7
  0.0 0.7 reshape.10.refs_8_
  0.7 0.7 reshape.11.refs_9_
  1.3 0.7 reshape.9.refs_1_
  2.0 0.0 copy-done.7
  2.0 0.0 copy-start
  2.0 1.2 %copy-done = bf16[2048,256]{1,0:T(8,128)(2,1)S(1)} copy-done((bf16[2048,256]{1,0:T(8,128)(2,1)S(1)}, bf16[2048,256]{1,0:T(8,128)(2,1)}, u32[]{:S(2)}) %copy-start) | copy-done | bytes 1048600
  3.3 0.0 copy-start.1
  3.3 1.2 %copy-done.1 = bf16[2048,256]{1,0:T(8,128)(2,1)S(1)} copy-done((bf16[2048,256]{1,0:T(8,128)(2,1)S(1)}, bf16[2048,256]{1,0:T(8,128)(2,1)}, u32[]{:S(2)}) %copy-start.1) | copy-done | bytes 1048600
  4.5 1.2 %copy-done.2 = bf16[2048,256]{1,0:T(8,128)(2,1)S(1)} copy-done((bf16[2048,256]{1,0:T(8,128)(2,1)S(1)}, bf16[2048,256]{1,0:T(8,128)(2,1)}, u32[]{:S(2)}) %copy-start.2) | copy-done | bytes 1048600
  5.7 0.0 copy-start.3
  5.7 1.0 %copy-done.3 = bf16[2048,128]{1,0:T(8,128)(2,1)S(1)} copy-done((bf16[2048,128]{1,0:T(8,128)(2,1)S(1)}, bf16[2048,128]{1,0:T(8,128)(2,1)}, u32[]{:S(2)}) %copy-start.3) | copy-done | bytes 524312
  6.8 0.0 copy-start.4
  6.8 1.0 %copy-done.4 = bf16[2048,128]{1,0:T(8,128)(2,1)S(1)} copy-done((bf16[2048,128]{1,0:T(8,128)(2,1)S(1)}, bf16[2048,128]{1,0:T(8,128)(2,1)}, u32[]{:S(2)}) %copy-start.4) | copy-done | bytes 524312
  7.8 0.0 copy-start.5
  7.8 0.9 %copy-done.5 = bf16[32,2048]{1,0:T(8,128)(2,1)S(1)} copy-done((bf16[32,2048]{1,0:T(8,128)(2,1)S(1)}, bf16[32,2048]{1,0:T(8,128)(2,1)}, u32[]{:S(2)}) %copy-start.5) | copy-done | bytes 131096
  8.7 0.0 copy-start.6
  8.7 0.9 %copy-done.6 = f32[16384,2]{0,1:T(2,128)S(1)} copy-done((f32[16384,2]{0,1:T(2,128)S(1)}, f32[16384,2]{0,1:T(2,128)}, u32[]{:S(2)}) %copy-start.6) | copy-done | bytes 131096
  9.6 0.0 copy-start.8
  9.6 0.7 copy-done.8
  10.3 0.0 copy-start.9
  10.3 0.7 copy-done.9
  11.0 69.0 %layer.1 = bf16[128,512]{1,0:T(8,128)(2,1)S(1)} custom-call(bf16[32,2048]{1,0:T(8,128)(2,1)S(1)} %copy-done.5, bf16[1,2048]{1,0:T(2,128)(2,1)S(1)} %reshape.9.refs_1_, bf16[2048,256]{1,0:T(8,128)(2,1)S(1)} %copy-done, bf16[2048,128]{1,0:T(8,128)(2,1)S(1)} %copy-done.3, bf16[2048,128]{1,0:T(8,128)(2,1)S(1)} %copy-done.4, bf16[2048,256]{1,0:T(8,128)(2,1)S(1)} %copy-done.1, ...), custom_call_target="tpu_custom_call" | custom-call | tf_op jit(solution)/shard_map/layer/pallas_call | solution.py:473
  80.0 0.7 copy.15
  (1 shorter events, 0.0 us)
Async XLA Ops:
  0.0 2.0 %copy-start.7 = (bf16[31,256]{1,0:T(8,128)(2,1)S(1)}, bf16[31,256]{1,0:T(8,128)(2,1)}, u32[]{:S(2)}) copy-start(bf16[31,256]{1,0:T(8,128)(2,1)} %refs_7_.1) | copy-start | bytes 47620
  2.0 1.2 %copy-start = (bf16[2048,256]{1,0:T(8,128)(2,1)S(1)}, bf16[2048,256]{1,0:T(8,128)(2,1)}, u32[]{:S(2)}) copy-start(bf16[2048,256]{1,0:T(8,128)(2,1)} %refs_2_.1) | copy-start | bytes 3145732
  3.3 1.2 %copy-start.1 = (bf16[2048,256]{1,0:T(8,128)(2,1)S(1)}, bf16[2048,256]{1,0:T(8,128)(2,1)}, u32[]{:S(2)}) copy-start(bf16[2048,256]{1,0:T(8,128)(2,1)} %refs_5_.1) | copy-start | bytes 3145732
  4.5 1.2 %copy-start.2 = (bf16[2048,256]{1,0:T(8,128)(2,1)S(1)}, bf16[2048,256]{1,0:T(8,128)(2,1)}, u32[]{:S(2)}) copy-start(bf16[2048,256]{1,0:T(8,128)(2,1)} %refs_6_.1) | copy-start | bytes 3145732
  5.7 1.0 %copy-start.3 = (bf16[2048,128]{1,0:T(8,128)(2,1)S(1)}, bf16[2048,128]{1,0:T(8,128)(2,1)}, u32[]{:S(2)}) copy-start(bf16[2048,128]{1,0:T(8,128)(2,1)} %refs_3_.1) | copy-start | bytes 1572868
  6.8 1.0 %copy-start.4 = (bf16[2048,128]{1,0:T(8,128)(2,1)S(1)}, bf16[2048,128]{1,0:T(8,128)(2,1)}, u32[]{:S(2)}) copy-start(bf16[2048,128]{1,0:T(8,128)(2,1)} %refs_4_.1) | copy-start | bytes 1572868
  7.8 0.9 %copy-start.5 = (bf16[32,2048]{1,0:T(8,128)(2,1)S(1)}, bf16[32,2048]{1,0:T(8,128)(2,1)}, u32[]{:S(2)}) copy-start(bf16[32,2048]{1,0:T(8,128)(2,1)} %refs_0_.1) | copy-start | bytes 393220
  8.7 0.9 %copy-start.6 = (f32[16384,2]{0,1:T(2,128)S(1)}, f32[16384,2]{0,1:T(2,128)}, u32[]{:S(2)}) copy-start(f32[16384,2]{0,1:T(2,128)} %param.23) | copy-start | bytes 393220
  9.6 0.7 copy-start.8
  10.3 0.7 copy-start.9

commit v2 on v1

v2 whole, which is shorter than its diff:
```python
import math

import jax
import jax.numpy as jnp
from jax import lax
from jax.experimental import pallas as pl
from jax.experimental.pallas import tpu as pltpu
from jax.sharding import PartitionSpec as P

HEAD = 128
KW = 31
ROWS = 128
LOG2E = math.log2(math.e)
FAR = 1e30
MESH = pl.DeviceIdType.MESH
F32 = jnp.float32
BF16 = jnp.bfloat16


def nt(a, b):
    return lax.dot_general(a, b, (((1,), (1,)), ((), ())), preferred_element_type=F32)


def nn(a, b):
    return lax.dot_general(a, b, (((1,), (0,)), ((), ())), preferred_element_type=F32)


SCOPE = []


def phase(name):
    if SCOPE:
        SCOPE.pop().__exit__(None, None, None)
    if name:
        scope = jax.named_scope(name)
        scope.__enter__()
        SCOPE.append(scope)


class Sems:
    def __init__(self, send, recv):
        self.send, self.recv, self.used = send, recv, 0

    def take(self, count=1):
        first = self.used
        self.used += count
        return first


class Ring:
    def __init__(self, n, sems, plus, minus, here, there):
        self.n, self.here, self.there = n, here, there
        self.peer = {1: plus, -1: minus}
        self.hops = n // 2
        self.base = sems.take(self.hops * 4)
        self.sems = sems
        self.started = []

    def index(self, way, k, ch):
        return self.base + ((k - 1) * 2 + (way < 0)) * 2 + ch

    def rel(self, way, k):
        return k if way > 0 else (self.n - k) % self.n

    def chunks(self, way, k):
        if k < self.hops:
            return (0, 1) if way > 0 else (1, 0)
        return (0,) if way > 0 else (1,)

    def start(self, way, k, ch):
        if k > self.hops or ch not in self.chunks(way, k):
            return
        i = self.index(way, k, ch)
        a, b = self.rel(way, k - 1), self.rel(way, k)
        c = pltpu.make_async_remote_copy(
            src_ref=self.here(a, ch),
            dst_ref=self.there(a, b, ch),
            send_sem=self.sems.send.at[i],
            recv_sem=self.sems.recv.at[i],
            device_id=self.peer[way],
            device_id_type=MESH,
        )
        c.start()
        self.started.append(c)

    def begin(self, chunks=(0, 1)):
        for n in range(2):
            for way in (1, -1):
                ch = n if way > 0 else 1 - n
                if ch in chunks:
                    self.start(way, 1, ch)

    def step(self, k, after=None):
        if k > self.hops:
            return
        for n in range(2):
            for way in (1, -1):
                ch = n if way > 0 else 1 - n
                if ch not in self.chunks(way, k):
                    continue
                i = self.index(way, k, ch)
                slot = self.here(self.rel(way, k), ch)
                pltpu.make_async_remote_copy(
                    src_ref=slot,
                    dst_ref=slot,
                    send_sem=self.sems.send.at[i],
                    recv_sem=self.sems.recv.at[i],
                    device_id=self.peer[-way],
                    device_id_type=MESH,
                ).wait_recv()
                self.start(way, k + 1, ch)
                if after is not None:
                    after(self.rel(way, k), ch)


def layer_kernel(
    nz, ny, nx,
    tokens_h, gain, wq, wk, wv, wcv, wcg, taps, cgain, cbias, gate_h, wa_t, wc_t,
    out,
    tokens, gate, tok_all, wbuf, qsend, qbuf, kv, conv_in, halo_out, halo_in, conv_s, st_out, st_in,
    wta, wtc, s_ref, peak_ref, gkb, o_out, o_in, rs_out, rs_in, proj_s, wsem, send, recv,
):
    rows = ROWS
    chip = 2 * rows
    dim = tokens.shape[1]
    trows = tokens.shape[0]
    chans = wcv.shape[1]
    ocols = out.shape[1]
    sp = lax.axis_index("sp")
    x = lax.axis_index("tp")
    c = lax.rem(sp, 2)
    y = lax.rem(lax.div(sp, 2), ny)
    z = lax.div(sp, 2 * ny)
    nsp = nz * ny * 2

    def at(zz, yy, cc):
        return (zz * ny + yy) * 2 + cc

    def mod(a, n):
        return lax.rem(a + 2 * n, n)

    sems = Sems(send, recv)
    pending = []

    def remote(src, dst, i, dev, ri=None):
        return pltpu.make_async_remote_copy(
            src_ref=src,
            dst_ref=dst,
            send_sem=send.at[i],
            recv_sem=recv.at[i if ri is None else ri],
            device_id=dev,
            device_id_type=MESH,
        )

    def launch(src, dst, i, dev, ri=None):
        cp = remote(src, dst, i, dev, ri)
        cp.start()
        pending.append(cp)

    def landed(slot, i, dev):
        remote(slot, slot, i, dev).wait_recv()

    sib = (at(z, y, 1 - c), x)
    y_up, y_down = (at(z, mod(y + 1, ny), c), x), (at(z, mod(y - 1, ny), c), x)
    z_up, z_down = (at(mod(z + 1, nz), y, c), x), (at(mod(z - 1, nz), y, c), x)
    x_up, x_down = (sp, mod(x + 1, nx)), (sp, mod(x - 1, nx))
    nxt, prv = mod(sp + 1, nsp), mod(sp - 1, nsp)

    phase("load")
    first = []
    for k, (a, b) in enumerate(
        ((tokens_h, tokens), (wa_t, wta.at[z, y, c]), (wc_t, wtc.at[z, y, c]), (gate_h, gate))
    ):
        cp = pltpu.make_async_copy(a, b, wsem.at[5 + k])
        cp.start()
        first.append(cp)
    wcols, off = [], 0
    for k, w in enumerate((wq, wk, wv, wcv, wcg)):
        cp = pltpu.make_async_copy(w, wbuf.at[:, off : off + w.shape[1]], wsem.at[k])
        cp.start()
        wcols.append(cp)
        off += w.shape[1]

    barrier = pltpu.get_barrier_semaphore()
    peers = [(sp, mod(x + d, nx)) for d in range(1, nx)]
    peers += [(at(z, mod(y + d, ny), cc), x) for d in range(1, ny) for cc in range(2)]
    peers += [(at(mod(z + d, nz), y, c), x) for d in range(1, nz)]
    peers += [sib, (nxt, x), (prv, x)]
    for p in peers:
        pl.semaphore_signal(barrier, inc=1, device_id=p, device_id_type=MESH)

    first[0].wait()
    tok = tokens[...].astype(F32)
    mean_sq = jnp.mean(tok * tok, axis=-1, keepdims=True)
    tok_all[x] = (tok * lax.rsqrt(mean_sq + 1e-06) * gain[...].astype(F32).reshape(1, dim)).astype(BF16)
    first[1].wait()
    first[2].wait()

    phase("barrier")
    pl.semaphore_wait(barrier, len(peers))

    phase("send_tok")
    th = trows // 2
    tr = Ring(
        nx, sems, x_up, x_down,
        lambda r, ch: tok_all.at[mod(x - r, nx), pl.ds(ch * th, th)],
        lambda a, b, ch: tok_all.at[mod(x - a, nx), pl.ds(ch * th, th)],
    )
    tr.begin()

    w1_i = sems.take(ny + nz)
    for d in sorted(range(1, ny), key=lambda d: -min(d, ny - d)):
        launch(wta.at[z, y, c], wta.at[z, y, c], w1_i + d, (at(z, mod(y + d, ny), c), x))
    for d in sorted(range(1, nz), key=lambda d: -min(d, nz - d)):
        launch(wtc.at[z, y, c], wtc.at[z, y, c], w1_i + ny + d, (at(mod(z + d, nz), y, c), x))
    yh, zh = ny // 2, nz // 2
    war = Ring(
        nz, sems, z_up, z_down,
        lambda r, ch: wta.at[mod(z - r, nz), pl.ds(ch * yh, yh), c],
        lambda a, b, ch: wta.at[mod(z - a, nz), pl.ds(ch * yh, yh), c],
    )
    wcr = Ring(
        ny, sems, y_up, y_down,
        lambda r, ch: wtc.at[pl.ds(ch * zh, zh), mod(y - r, ny), c],
        lambda a, b, ch: wtc.at[pl.ds(ch * zh, zh), mod(y - a, ny), c],
    )
    was_i, wcs_i = sems.take(2 * nz), sems.take(2 * ny)

    def pass_wa(rel, ch):
        slot = war.here(rel, ch)
        launch(slot, slot, was_i + 2 * rel + ch, sib)

    def pass_wc(rel, ch):
        slot = wcr.here(rel, ch)
        launch(slot, slot, wcs_i + 2 * rel + ch, sib)

    def w_step(k):
        war.step(k, pass_wa)
        wcr.step(k, pass_wc)

    def core_rows(ch):
        return pl.ds(pl.multiple_of((c if ch == 0 else 1 - c) * rows, rows), rows)

    qr = Ring(
        ny, sems, y_up, y_down,
        lambda r, ch: qbuf.at[r, core_rows(ch)],
        lambda a, b, ch: qbuf.at[b, core_rows(ch)],
    )
    kr = Ring(
        nz, sems, z_up, z_down,
        lambda r, ch: kv.at[r, 0, pl.ds(ch * rows, rows)],
        lambda a, b, ch: kv.at[b, 0, pl.ds(ch * rows, rows)],
    )
    ks_i = sems.take(2 * nz)

    def pass_kv(rel, ch):
        part = pl.ds(ch * rows, rows)
        launch(kv.at[rel, 0, part], kv.at[rel, 1, part], ks_i + 2 * rel + ch, sib)

    def wait_kv(rel, ch):
        landed(kv.at[rel, 1, pl.ds(ch * rows, rows)], ks_i + 2 * rel + ch, sib)

    phase("gates")
    first[3].wait()
    g_first = gate[:, pl.ds(pl.multiple_of(z * ny * chip, chip), 128)]
    g_ref = jnp.where(c == 0, g_first[0:1, 0:1], g_first[1:2, 0:1])

    def gate_row(start, width):
        g = gate[:, pl.ds(pl.multiple_of(start, 128), width)]
        return (jnp.where(c == 0, g[0:1], g[1:2]) - g_ref) * LOG2E

    for s in range(nz):
        for p in range(2):
            cc = c if p == 0 else 1 - c
            g = gate_row(at(mod(z - s, nz), y, cc) * rows, rows)
            g = jnp.where(s <= z, g, FAR)
            gkb[pl.ds((s * 2 + p) * rows, rows), :] = jnp.transpose(jnp.broadcast_to(g, (128, rows)))
    for r in range(ny):
        peak_ref[r] = jnp.full((8, chip), -FAR, F32)

    phase("tok1")
    tr.step(1)
    phase("w1")
    for d in range(1, ny):
        yy = mod(y - d, ny)
        landed(wta.at[z, yy, c], w1_i + d, (at(z, yy, c), x))
    for d in range(1, nz):
        zz = mod(z - d, nz)
        landed(wtc.at[zz, y, c], w1_i + ny + d, (at(zz, y, c), x))
    war.begin()
    wcr.begin()
    phase("wait_w")
    for cp in wcols[:3]:
        cp.wait()
    phase("tok2")
    for k in range(2, nx // 2 + 1):
        tr.step(k)

    phase("qkv")
    normed = tok_all[...].reshape(rows, dim)
    qw, kw_ = wq.shape[1], wk.shape[1]
    qkv = nn(normed, wbuf[:, : qw + 2 * kw_])
    q0 = qkv[:, :HEAD].astype(BF16)
    q1 = qkv[:, HEAD:qw].astype(BF16)
    kv[0, 0, :rows] = qkv[:, qw : qw + kw_].astype(BF16)
    kv[0, 0, rows:] = jnp.transpose(qkv[:, qw + kw_ :]).astype(BF16)
    mine = core_rows(0)
    qbuf[0, mine] = jnp.where(c == 0, q0, q1)
    qsend[...] = jnp.where(c == 0, q1, q0)

    q_i = sems.take()
    launch(qsend, qbuf.at[0, mine], q_i, sib)
    kr.begin()
    qr.begin((0,))
    for ch in range(2):
        pass_kv(0, ch)

    phase("glu")
    for cp in wcols[3:]:
        cp.wait()
    halves = nn(normed, wbuf[:, qw + 2 * kw_ :])
    phase("wait_qsib")
    landed(qbuf.at[0, core_rows(1)], q_i, sib)
    qr.begin((1,))
    phase("glu2")
    glu = (halves[:, :chans] * jax.nn.sigmoid(halves[:, chans:])).astype(BF16)
    conv_in[32:] = glu.astype(F32)
    halo_out[...] = glu[rows - 32 :]
    h_i = sems.take()
    launch(halo_out, halo_in, h_i, (nxt, x))
    for ch in range(2):
        for rel in range(1):
            pass_wa(rel, ch)
            pass_wc(rel, ch)

    scale = LOG2E / math.sqrt(HEAD)
    key_lo = lax.broadcasted_iota(jnp.int32, (rows, chip), 0)
    q_at = lax.broadcasted_iota(jnp.int32, (rows, chip), 1)
    done = set()

    def logits(q_slots, k_slots):
        for r in q_slots:
            parts = [(s, p) for s, p in k_slots if (r, s, p) not in done]
            done.update((r, s, p) for s, p in parts)
            if not parts:
                continue
            all_t = nt(jnp.concatenate([kv[s, p, :rows] for s, p in parts], axis=0), qbuf[r])
            peak = peak_ref[r]
            for n, (s, p) in enumerate(parts):
                own = pl.ds((s * 2 + p) * rows, rows)
                g = gkb[own, :]
                t = all_t[n * rows : (n + 1) * rows] * scale - jnp.concatenate([g, g], axis=1)
                if s == 0:
                    cc = c if p == 0 else 1 - c
                    shift = (y - mod(y - r, ny)) * chip + cc * rows
                    t = jnp.where(key_lo + shift <= q_at, t, -FAR)
                s_ref[r, own, :] = t
                peak = jnp.maximum(peak, jnp.max(t.reshape(rows // 8, 8, chip), axis=0))
            peak_ref[r] = peak

    def near(n, k):
        return sorted({d % n for d in range(-min(k, n // 2), min(k, n // 2) + 1)})

    got = set()

    def hop(k):
        qr.step(k)
        kr.step(k, pass_kv)

    def catch_up(k):
        own = [(s, 0) for s in near(nz, k)]
        for s in near(nz, k - 1):
            if s not in got:
                wait_kv(s, 0)
                got.add(s)
        logits(near(ny, k), own + [(s, 1) for s in sorted(got)])

    phase("hop1")
    hop(1)
    phase("w_hop1")
    w_step(1)
    phase("conv_in")
    landed(halo_in, h_i, (prv, x))
    conv_in[:32] = jnp.where(sp == 0, 0.0, halo_in[...].astype(F32))
    tap = taps[...].astype(F32)
    half = KW // 2
    conv = jnp.zeros((rows, chans), F32)
    for k in range(half):
        conv = conv + tap[k : k + 1] * conv_in[2 + k : 2 + k + rows]
    conv_s[...] = conv
    phase("logits1")
    catch_up(1)
    phase("hop2")
    hop(2)
    phase("conv2")
    conv = conv_s[...]
    for k in range(half, KW):
        conv = conv + tap[k : k + 1] * conv_in[2 + k : 2 + k + rows]
    conv_s[...] = conv
    s1 = jnp.sum(conv, axis=1, keepdims=True)
    s2 = jnp.sum(conv * conv, axis=1, keepdims=True)
    lane = lax.broadcasted_iota(jnp.int32, (rows, 128), 1)
    st_out[...] = jnp.transpose(jnp.where(lane == 0, s1, s2))[:8]
    st_i = sems.take(nx)
    for d in range(1, nx):
        launch(st_out, st_in.at[nx - d], st_i + d, (sp, mod(x + d, nx)))
    phase("logits2")
    catch_up(2)
    phase("hop3")
    hop(3)
    phase("logits3")
    catch_up(3)
    phase("hop4")
    for k in range(4, max(ny, nz) // 2 + 1):
        hop(k)
    phase("w_hop2")
    w_step(2)
    phase("logits4")
    catch_up(max(ny, nz) // 2)
    phase("wait_kvsib")
    catch_up(max(ny, nz) // 2 + 1)
    for s in range(nz):
        wait_kv(s, 1)

    ones = jnp.ones((16, chip), BF16)
    o_i = sems.take(ny * 2)
    sub = lax.broadcasted_iota(jnp.int32, (16, rows), 0)

    def attend(r):
        jq = mod(y - r, ny)
        m = jnp.max(peak_ref[r], axis=0, keepdims=True)
        acc = jnp.zeros((HEAD + 16, chip), F32)
        for s in range(nz):
            w = jnp.exp2(s_ref[r, pl.ds(s * chip, chip), :] - m).astype(BF16)
            vt = jnp.concatenate([kv[s, 0, rows:], kv[s, 1, rows:]], axis=1)
            acc = acc + nn(jnp.concatenate([vt, ones], axis=0), w)
        den = acc[HEAD : HEAD + 1]
        o = (acc[:HEAD] / den).astype(BF16)
        m = m + gate_row((z * ny + jq) * chip, chip)
        m1 = m.astype(BF16).astype(F32)
        m2 = (m - m1).astype(BF16).astype(F32)
        d1 = den.astype(BF16).astype(F32)
        d2 = (den - d1).astype(BF16).astype(F32)
        parts = (m1, m2, m - m1 - m2, d1, d2, den - d1 - d2)
        for cc in range(2):
            lanes = slice(cc * rows, (cc + 1) * rows)
            tile = jnp.zeros((16, rows), F32)
            for i, part in enumerate(parts):
                tile = jnp.where(sub == i, part[:, lanes], tile)
            o_out[r, cc, :HEAD] = o[:, lanes]
            o_out[r, cc, HEAD:] = tile.astype(BF16)

    ring_order = sorted(range(ny), key=lambda r: (-min(r, ny - r), r))
    for n, r in enumerate(ring_order):
        phase(f"attend{n}")
        attend(r)
        phase(f"sendo{n}")
        if r:
            for cc in range(2):
                launch(
                    o_out.at[r, cc], o_in.at[r, c], o_i + 2 * r + cc, (at(z, mod(y - r, ny), cc), x), o_i + 2 * r + c
                )
        if n == ny // 2 - 1:
            w_step(3)
    launch(o_out.at[0, 1 - c], o_in.at[0, c], o_i + 1 - c, sib, o_i + c)

    phase("chan_norm")
    tot = st_out[...]
    for d in range(1, nx):
        landed(st_in.at[nx - d], st_i + d, (sp, mod(x - d, nx)))
        tot = tot + st_in[nx - d]
    total_chans = chans * nx
    mean_r = tot[0:1] / total_chans
    var_r = tot[1:2] / total_chans - mean_r * mean_r
    rstd_r = lax.rsqrt(var_r + 1e-05)
    mean_c = jnp.transpose(jnp.broadcast_to(mean_r, (128, rows)))
    rstd_c = jnp.transpose(jnp.broadcast_to(rstd_r, (128, rows)))
    wide = chans // 128
    mean_c = jnp.concatenate([mean_c] * wide, axis=1)
    rstd_c = jnp.concatenate([rstd_c] * wide, axis=1)
    shaped = (conv_s[...] - mean_c) * rstd_c * cgain[...].astype(F32).reshape(1, chans)
    shaped = shaped + cbias[...].astype(F32).reshape(1, chans)
    conv_act = (shaped / (1.0 + jnp.exp(-shaped))).astype(BF16)

    phase("w_hop4")
    for k in range(4, max(ny, nz) // 2 + 1):
        w_step(k)
    phase("wait_wsib")
    for s in range(nz):
        for ch in range(2):
            slot = wta.at[mod(z - s, nz), pl.ds(ch * yh, yh), 1 - c]
            landed(slot, was_i + 2 * s + ch, sib)
    for s in range(ny):
        for ch in range(2):
            slot = wtc.at[pl.ds(ch * zh, zh), mod(y - s, ny), 1 - c]
            landed(slot, wcs_i + 2 * s + ch, sib)
    phase("proj_conv")
    per = nz // nx
    for d in range(nx):
        xx = mod(x + d, nx)
        w = wtc[pl.ds(xx * per, per)].reshape(ocols, chans)
        proj_s[d] = nt(conv_act, w)

    phase("wait_o")
    o_in[0, c] = o_out[0, c]
    for r in range(1, ny):
        for hh in range(2):
            landed(o_in.at[r, hh], o_i + 2 * r + hh, (at(z, mod(y + r, ny), hh), x))
    landed(o_in.at[0, 1 - c], o_i + 1 - c, sib)
    phase("merge")
    heads = []
    for hh in range(2):
        tiles = [o_in[r, hh, HEAD:].astype(F32) for r in range(ny)]
        tops = [t[0:1] + t[1:2] + t[2:3] for t in tiles]
        dens = [t[3:4] + t[4:5] + t[5:6] for t in tiles]
        top = tops[0]
        for t in tops[1:]:
            top = jnp.maximum(top, t)
        scaled = [d * jnp.exp2(t - top) for d, t in zip(dens, tops)]
        den = scaled[0]
        for d in scaled[1:]:
            den = den + d
        acc = jnp.zeros((HEAD, rows), F32)
        for r in range(ny):
            acc = acc + o_in[r, hh, :HEAD].astype(F32) * (scaled[r] / den)
        heads.append(jnp.transpose(acc).astype(BF16))
    attended = jnp.concatenate(heads, axis=1)

    phase("proj_att")
    rs_i = sems.take(nx)
    for d in sorted(range(1, nx), key=lambda d: -min(d, nx - d)) + [0]:
        xx = mod(x + d, nx)
        w = wta[pl.ds(xx * per, per)].reshape(ocols, wta.shape[4])
        part = proj_s[d] + nt(attended, w)
        if d:
            rs_out[d] = part.astype(BF16)
            launch(rs_out.at[d], rs_in.at[d], rs_i + d, (sp, xx))
        else:
            total = part
    phase("wait_rs")
    for d in range(1, nx):
        landed(rs_in.at[d], rs_i + d, (sp, mod(x - d, nx)))
        total = total + rs_in[d].astype(F32)
    out[...] = total.astype(BF16)

    phase("wait_send")
    for cp in pending:
        cp.wait_send()
    for ring in (tr, war, wcr, qr, kr):
        for cp in ring.started:
            cp.wait_send()
    phase(None)


def layer(nz, ny, nx, *args):
    (tokens, gain, wq, wk, wv, wcv, wcg, taps, cgain, cbias, cum_gate, wa, wc) = args
    dim = tokens.shape[1]
    trows = tokens.shape[0]
    rows, chip = ROWS, 2 * ROWS
    nsp = nz * ny * 2
    chans = wcv.shape[1]
    wcol = wa.shape[1]
    cols = wq.shape[1] + wk.shape[1] + wv.shape[1] + wcv.shape[1] + wcg.shape[1]
    ocols = wcol * nsp // nx
    vm = pl.BlockSpec(memory_space=pltpu.VMEM)
    hb = pl.BlockSpec(memory_space=pltpu.HBM)
    nsem = 4 * nx + 9 * ny + 9 * nz + 2
    scratch = [
        pltpu.VMEM((trows, dim), BF16),
        pltpu.VMEM((2, nsp * rows), F32),
        pltpu.VMEM((nx, trows, dim), BF16),
        pltpu.VMEM((dim, cols), BF16),
        pltpu.VMEM((rows, HEAD), BF16),
        pltpu.VMEM((ny, chip, HEAD), BF16),
        pltpu.VMEM((nz, 2, rows + HEAD, 128), BF16),
        pltpu.VMEM((32 + rows, chans), F32),
        pltpu.VMEM((32, chans), BF16),
        pltpu.VMEM((32, chans), BF16),
        pltpu.VMEM((rows, chans), F32),
        pltpu.VMEM((8, 128), F32),
        pltpu.VMEM((nx, 8, 128), F32),
        pltpu.VMEM((nz, ny, 2, wcol, 256), BF16),
        pltpu.VMEM((nz, ny, 2, wcol, 256), BF16),
        pltpu.VMEM((ny, nz * chip, chip), F32),
        pltpu.VMEM((ny, 8, chip), F32),
        pltpu.VMEM((nz * chip, 128), F32),
        pltpu.VMEM((ny, 2, HEAD + 16, rows), BF16),
        pltpu.VMEM((ny, 2, HEAD + 16, rows), BF16),
        pltpu.VMEM((nx, rows, ocols), BF16),
        pltpu.VMEM((nx, rows, ocols), BF16),
        pltpu.VMEM((nx, rows, ocols), F32),
        pltpu.SemaphoreType.DMA((9,)),
        pltpu.SemaphoreType.DMA((nsem,)),
        pltpu.SemaphoreType.DMA((nsem,)),
    ]

    def kernel(*refs):
        layer_kernel(nz, ny, nx, *refs)

    return pl.pallas_call(
        kernel,
        out_shape=jax.ShapeDtypeStruct((rows, ocols), BF16),
        in_specs=[hb, vm, hb, hb, hb, hb, hb, vm, vm, vm, hb, hb, hb],
        out_specs=vm,
        scratch_shapes=scratch,
        compiler_params=pltpu.CompilerParams(
            collective_id=0, has_side_effects=True, vmem_limit_bytes=60 * 1024 * 1024
        ),
        name="layer",
    )(
        tokens, gain, wq, wk, wv, wcv, wcg, taps, cgain, cbias, cum_gate.T, wa.T, wc.T
    )


def build(mesh, nz, ny):
    nx = mesh.shape["tp"]

    def shards(*args):
        return layer(nz, ny, nx, *args)

    return jax.shard_map(
        shards,
        mesh=mesh,
        in_specs=(
            P(("sp", "tp"), None),
            P(),
            P(None, "tp"),
            P(None, "tp"),
            P(None, "tp"),
            P(None, "tp"),
            P(None, "tp"),
            P(None, "tp"),
            P("tp"),
            P("tp"),
            P(None, "tp"),
            P("tp", "sp"),
            P("tp", "sp"),
        ),
        out_specs=P("sp", "tp"),
        check_vma=False,
    )


def solution(mesh):
    side = math.isqrt(mesh.shape["sp"] // 2)
    return build(mesh, side, side)
```

time: 81.2 us -> 71.5 us (0.88)
  local copies, waits for them, and re-layouts: 11.6 us -> 1.57 us
    unnamed x21 -> x1, local copies, waits for them, and re-layouts: 9.61 us -> 1.57 us
    reshape x3 -> x0, local copies, waits for them, and re-layouts: 2.02 us -> none  [the longest x1 0.69 us: layer(): gain.reshape(1, dim)]
where the time goes in v2:
time: 71.5 us; the launch traced here: 71.3 us
  Pallas kernels  69.8 us (98%)
  local copies, waits for them, and re-layouts  1.57 us (2%)
    pallas_call x1, Pallas kernels, layer(): pl.pallas_call(kernel, out_shape=jax.ShapeDtypeStruct((rows, ocols), BF16...  69.8 us
    unnamed x1, local copies, waits for them, and re-layouts  1.57 us

profile of v2, /device:TPU:1, one launch (start us, length us, event | category | flops | bytes accessed | tf_op | source)
XLA Modules:
  0.0 71.3 jit_solution(17113753063438529392)
XLA Ops:
  0.0 69.8 %layer.1 = bf16[128,512]{1,0:T(8,128)(2,1)} custom-call(bf16[32,2048]{1,0:T(8,128)(2,1)} %refs_0_.1, bf16[2048]{0:T(1024)(128)(2,1)} %refs_1_.1, bf16[2048,256]{1,0:T(8,128)(2,1)} %refs_2_.1, bf16[2048,128]{1,0:T(8,128)(2,1)} %refs_3_.1, bf16[2048,128]{1,0:T(8,128)(2,1)} %refs_4_.1, bf16[2048,256]{1,0:T(8,128)(2,1)} %refs_5_.1, bf16[2048,256]{1,0:T(8,128)(2,1)} %refs_6_.1, ...), custom_call_target="tpu_custom_call" | custom-call | tf_op jit(solution)/shard_map/layer/pallas_call | solution.py:600
  69.8 1.6 %copy.15 = bf16[128,512]{1,0:T(8,128)(2,1)} copy(bf16[128,512]{1,0:T(8,128)(2,1)} %layer.1) | data formatting | bytes 262144
